TPU v7x, 32 devices: a whole 2x2x4 slice. The times are simulated.
32 devices in a mesh: sp: 8 (over z, y), tp: 4 (over x, core).
Axes of the slice: x: 2, y: 2, z: 4, core: 2. Of those that a mesh axis runs over, the one named last changes fastest.
Arguments:
- hidden_in: bfloat16 [6144, 4096], P('sp', 'tp'), may hold values from -16 to 16
- norm_gain: bfloat16 [2, 4096], P(None, 'tp'), may hold values from 0.099609375 to 1.8984375
- value_proj: bfloat16 [2, 4096, 1024], P(None, 'tp', 'sp'), may hold values from -0.09375 to 0.09375
- gate_proj: bfloat16 [2, 4096, 1024], P(None, 'tp', 'sp'), may hold values from -0.09375 to 0.09375
- conv_taps: bfloat16 [2, 31, 1024], P(None, None, 'tp'), may hold values from -1 to 1
- conv_bias: bfloat16 [2, 1024], P(None, 'tp'), may hold values from -3 to 3
- group_gain: bfloat16 [2, 1024], P(None, 'tp'), may hold values from 0.099609375 to 1.8984375
- group_shift: bfloat16 [2, 1024], P(None, 'tp'), may hold values from -3 to 3
- out_proj: bfloat16 [2, 1024, 4096], P(None, 'sp', 'tp'), may hold values from -0.1875 to 0.1875
Outputs:
- hidden_out: bfloat16 [6144, 4096], P('sp', 'tp')
All inputs are finite; a program needn't handle non-finite values.
Results may differ from a plain program's by a relative error of at most 0.012.
Values may be sent and summed in bfloat16 or wider, within the bound.
A program may use at most 128 MiB of HBM per device.

v0:
```python
import jax
import jax.numpy as jnp
from jax import lax
from jax.sharding import PartitionSpec as P

D = 4096
C = 1024
GROUPS = 4
WIDTH = 31
row_floor = 1e-06
group_floor = 1e-05


def passed_along(value, axis, steps):
    count = lax.axis_size(axis)
    initial, last = (max(0, -steps), min(count, count - steps))
    return lax.ppermute(value, axis, [(source, source + steps) for source in range(initial, last)])


def rms_normed(residual_rows, gain_part):
    wide_rows = residual_rows.astype(jnp.float32)
    squares = lax.psum(jnp.sum(wide_rows * wide_rows, axis=1), "tp")
    scale_rows = lax.rsqrt(squares / D + row_floor)
    return (wide_rows * scale_rows[:, None] * gain_part.astype(jnp.float32)[None, :]).astype(
        jnp.bfloat16
    )


def gated_input(normed_rows, w_value, w_gate):
    numbers = (((0,), (1,)), ((), ()))
    value_part = lax.dot_general(w_value, normed_rows, numbers, preferred_element_type=jnp.float32)
    gate_part = lax.dot_general(w_gate, normed_rows, numbers, preferred_element_type=jnp.float32)
    summed = lax.psum_scatter(
        jnp.stack([value_part, gate_part], axis=1).astype(jnp.bfloat16),
        "tp",
        scatter_dimension=0,
        tiled=True,
    ).astype(jnp.float32)
    return (summed[:, 0] * jax.nn.sigmoid(summed[:, 1])).astype(jnp.bfloat16)


def depthwise(extended, taps_part, bias_part, out_len):
    widened = extended.astype(jnp.float32)
    taps = taps_part.astype(jnp.float32)
    filtered = (
        jnp.zeros((extended.shape[0], out_len), jnp.float32)
        + bias_part.astype(jnp.float32)[:, None]
    )
    for offset in range(WIDTH):
        filtered = filtered + taps[offset][:, None] * widened[:, offset : offset + out_len]
    return filtered


def group_normed(filtered, gain_part, shift_part, group_size):
    channels, out_len = filtered.shape
    grouped = filtered.reshape(channels // group_size, group_size, out_len)
    group_mean = jnp.mean(grouped, axis=1, keepdims=True)
    centered = grouped - group_mean
    group_var = jnp.mean(centered * centered, axis=1, keepdims=True)
    scaled = (centered * lax.rsqrt(group_var + group_floor)).reshape(channels, out_len)
    scaled = (
        scaled * gain_part.astype(jnp.float32)[:, None] + shift_part.astype(jnp.float32)[:, None]
    )
    return jax.nn.silu(scaled).astype(jnp.bfloat16)


def project_out(mixed, w_out):
    return lax.dot_general(
        lax.all_gather(mixed, "tp", axis=0, tiled=True),
        w_out,
        (((0,), (0,)), ((), ())),
        preferred_element_type=jnp.float32,
    )


def on_device(
    hidden_in,
    norm_gain,
    value_proj,
    gate_proj,
    conv_taps,
    conv_bias,
    group_gain,
    group_shift,
    out_proj,
):
    tok_rows = hidden_in.shape[0]
    layers = norm_gain.shape[0]
    reach_back = WIDTH - 1
    group_size = C // GROUPS
    all_value, all_gate, all_out = (
        lax.all_gather(value_proj, "sp", axis=2, tiled=True),
        lax.all_gather(gate_proj, "sp", axis=2, tiled=True),
        lax.all_gather(out_proj, "sp", axis=1, tiled=True),
    )
    residual_rows = hidden_in
    for level in range(layers):
        w_value, w_gate, w_out = (all_value[level], all_gate[level], all_out[level])
        normed_rows = rms_normed(residual_rows, norm_gain[level])
        gated = gated_input(normed_rows, w_value, w_gate)
        before = passed_along(gated[:, tok_rows - reach_back :], "sp", 1)
        extended = jnp.concatenate([before, gated], axis=1)
        out_len = extended.shape[1] - reach_back
        filtered = depthwise(extended, conv_taps[level], conv_bias[level], out_len)
        mixed = group_normed(filtered, group_gain[level], group_shift[level], group_size)
        update = project_out(mixed, w_out)
        kept_rows = residual_rows
        residual_rows = (kept_rows.astype(jnp.float32) + update).astype(jnp.bfloat16)
    return residual_rows


def solution(mesh):
    return jax.shard_map(
        on_device,
        mesh=mesh,
        in_specs=(
            P("sp", "tp"),
            P(None, "tp"),
            P(None, "tp", "sp"),
            P(None, "tp", "sp"),
            P(None, None, "tp"),
            P(None, "tp"),
            P(None, "tp"),
            P(None, "tp"),
            P(None, "sp", "tp"),
        ),
        out_specs=P("sp", "tp"),
        check_vma=False,
    )
```

profile of v0, /device:TPU:0, one launch (start us, length us, event | category | flops | bytes accessed | tf_op | source)
XLA Modules:
  0.0 397.9 jit_solution(1611705756857018403)
XLA Ops:
  6.5 0.7 all-gather.8.cloned.1.call-update
  7.3 0.7 all-gather.6.cloned.1.call-update
  8.1 1.8 fusion
  9.8 8.4 %psum.14 = f32[768]{0:T(1024)S(1)} all-reduce(f32[768]{0:T(1024)S(1)} %fusion), channel_id=1, replica_groups=mesh['sp'=8,'tp'=4] {'tp'}, use_global_device_ids=true, to_apply=%region_1.0 | all-reduce | flops 768 | bytes 6144 | tf_op jit(solution)/shard_map/psum | solution.py:22
  18.2 68.5 %all-gather.8.cloned.1.call-done = bf16[2,1024,1024]{2,1,0:T(8,128)(2,1)} async-done(((bf16[2,1024,128]{2,1,0:T(8,128)(2,1)}), bf16[2,1024,1024]{2,1,0:T(8,128)(2,1)}) %all-gather.8.cloned.1.call-update) | async-done | bytes 4194320 | tf_op jit(solution)/shard_map/all_gather | solution.py:93
  86.8 3.4 fusion.20
  90.2 71.4 %all-gather.6.cloned.1.call-done = bf16[2,1024,1024]{2,1,0:T(8,128)(2,1)} async-done(((bf16[2,1024,128]{2,1,0:T(8,128)(2,1)}), bf16[2,1024,1024]{2,1,0:T(8,128)(2,1)}) %all-gather.6.cloned.1.call-update) | async-done | bytes 4194320 | tf_op jit(solution)/shard_map/all_gather | solution.py:92
  161.7 3.4 fusion.21
  165.1 1.9 pad_maximum_fusion
  167.1 0.5 all-gather.12.cloned.1.call-update
  167.9 35.2 %reduce-scatter.3.cloned.1.call-done = bf16[256,2,768]{0,2,1:T(8,128)(2,1)} async-done(((bf16[1024,2,768]{0,2,1:T(8,128)(2,1)}), bf16[256,2,768]{0,2,1:T(8,128)(2,1)}) %reduce-scatter.3.cloned.1.call-update) | async-done | bytes 786448 | tf_op jit(solution)/shard_map/reduce_scatter | solution.py:33
  203.1 1.2 convert_element_type.123
  204.6 3.4 collective-permute-start
  208.0 1.4 collective-permute-done
  209.5 3.3 fusion.102
  213.1 1.1 multiply_convert_fusion.1
  214.3 63.7 %all-gather.12.cloned.1.call-done = bf16[2,1024,1024]{2,1,0:T(8,128)(2,1)} async-done(((bf16[2,128,1024]{2,1,0:T(8,128)(2,1)}), bf16[2,1024,1024]{2,1,0:T(8,128)(2,1)}) %all-gather.12.cloned.1.call-update) | async-done | bytes 4194320 | tf_op jit(solution)/shard_map/all_gather | solution.py:94
  278.0 19.8 %all-gather.10.cloned.1.call-done = bf16[1024,768]{0,1:T(8,128)(2,1)} async-done(((bf16[256,768]{0,1:T(8,128)(2,1)}), bf16[1024,768]{0,1:T(8,128)(2,1)}) %all-gather.10.cloned.1.call-update) | async-done | bytes 1572880 | tf_op jit(solution)/shard_map/all_gather | solution.py:69
  297.7 4.1 %fusion.4 = (f32[768]{0:T(1024)S(1)}, bf16[768,1024]{1,0:T(8,128)(2,1)S(1)}) fusion(bf16[1024,768]{0,1:T(8,128)(2,1)} %all-gather.10.cloned.1.call-done, bf16[2,1024,1024]{2,1,0:T(8,128)(2,1)} %all-gather.12.cloned.1.call-done, bf16[768,1024]{1,0:T(8,128)(2,1)S(1)} %copy-done), kind=kOutput, calls=%fused_computation.10 | convolution fusion | flops 1615330560 | bytes 6818816 | tf_op jit(solution)/shard_map/dot_general | solution.py:68
  301.8 5.9 %psum.15 = f32[768]{0:T(1024)S(1)} all-reduce(f32[768]{0:T(1024)S(1)} %get-tuple-element.81), channel_id=1, replica_groups=mesh['sp'=8,'tp'=4] {'tp'}, use_global_device_ids=true, to_apply=%region_6.7 | all-reduce | flops 768 | bytes 6144 | tf_op jit(solution)/shard_map/psum | solution.py:22
  307.7 3.6 fusion.19
  311.3 1.9 fusion.18
  313.2 2.0 pad_maximum_fusion.1
  315.2 38.9 %reduce-scatter.5.cloned.1.call-done = bf16[256,2,768]{0,2,1:T(8,128)(2,1)} async-done(((bf16[1024,2,768]{0,2,1:T(8,128)(2,1)}), bf16[256,2,768]{0,2,1:T(8,128)(2,1)}) %reduce-scatter.5.cloned.1.call-update) | async-done | bytes 786448 | tf_op jit(solution)/shard_map/reduce_scatter | solution.py:33
  354.1 1.2 convert_element_type.137
  355.6 3.4 collective-permute-start.1
  359.0 1.4 collective-permute-done.1
  360.5 3.3 fusion.100
  363.8 0.3 multiply_reduce_fusion
  364.1 1.1 multiply_convert_fusion
  365.2 20.8 %all-gather.14.cloned.1.call-done = bf16[1024,768]{0,1:T(8,128)(2,1)} async-done(((bf16[256,768]{0,1:T(8,128)(2,1)}), bf16[1024,768]{0,1:T(8,128)(2,1)}) %all-gather.14.cloned.1.call-update) | async-done | bytes 1572880 | tf_op jit(solution)/shard_map/all_gather | solution.py:69
  386.0 5.0 %fusion.7 = bf16[768,1024]{1,0:T(8,128)(2,1)} fusion(bf16[768,1024]{1,0:T(8,128)(2,1)S(1)} %get-tuple-element.82, bf16[1024,768]{0,1:T(8,128)(2,1)} %all-gather.14.cloned.1.call-done, bf16[2,1024,1024]{2,1,0:T(8,128)(2,1)} %all-gather.12.cloned.1.call-done), kind=kOutput, calls=%fused_computation.13 | convolution fusion | flops 1612972032 | bytes 6815744 | tf_op jit(solution)/shard_map/dot_general | solution.py:68
  (47 shorter events, 1.5 us)
Async XLA Ops:
  6.5 80.2 %copy-start = (bf16[768,1024]{1,0:T(8,128)(2,1)S(1)}, bf16[768,1024]{1,0:T(8,128)(2,1)}, u32[]{:S(2)}) copy-start(bf16[768,1024]{1,0:T(8,128)(2,1)} %param.9) | copy-start | bytes 4718596
  6.5 11.7 %copy-start.2 = (bf16[2,1024]{1,0:T(2,128)(2,1)S(1)}, bf16[2,1024]{1,0:T(2,128)(2,1)}, u32[]{:S(2)}) copy-start(bf16[2,1024]{1,0:T(2,128)(2,1)} %param.10) | copy-start | bytes 12292
  6.5 80.2 %all-gather.8.cloned.1.call-start = ((), (), s32[]{:S(2)}) async-start(), calls=%async_computation.3 | async-start | bytes 4718592 | tf_op jit(solution)/shard_map/all_gather | solution.py:93
  7.3 154.4 %all-gather.6.cloned.1.call-start = ((), (), s32[]{:S(2)}) async-start(), calls=%async_computation.2 | async-start | bytes 4718592 | tf_op jit(solution)/shard_map/all_gather | solution.py:92
  8.0 195.1 %reduce-scatter.3.cloned.1.call-start = ((), (), s32[]{:S(2)}) async-start(), calls=%async_computation.4 | async-start | bytes 3932160 | tf_op jit(solution)/shard_map/reduce_scatter | solution.py:33
  167.0 0.7 copy-start.3
  167.0 0.7 copy-start.4
  167.0 0.8 copy-start.1
  167.1 110.9 %all-gather.12.cloned.1.call-start = ((), (), s32[]{:S(2)}) async-start(), calls=%async_computation.6 | async-start | bytes 4718592 | tf_op jit(solution)/shard_map/all_gather | solution.py:94
  167.6 130.1 %all-gather.10.cloned.1.call-start = ((), (), s32[]{:S(2)}) async-start(), calls=%async_computation.5 | async-start | bytes 1966080 | tf_op jit(solution)/shard_map/all_gather | solution.py:69
  167.9 40.1 %copy-start.5 = (bf16[2,256]{1,0:T(2,128)(2,1)S(1)}, bf16[2,256]{1,0:T(2,128)(2,1)}, u32[]{:S(2)}) copy-start(bf16[2,256]{1,0:T(2,128)(2,1)} %param.16) | copy-start | bytes 3076
  204.6 4.8 %collective-permute-start = (bf16[256,30]{0,1:T(8,128)(2,1)S(1)}, bf16[256,30]{0,1:T(8,128)(2,1)S(1)}, u32[]{:S(2)}, u32[]{:S(2)}) collective-permute-start(bf16[256,30]{0,1:T(8,128)(2,1)S(1)} %slice.651), channel_id=1, source_target_pairs={{0,4},{4,8},{8,12},{12,16},{16,20},{20,24},{24,28},{1,5},{5,9},{9,... | collective-permute-start | bytes 46088 | tf_op jit(solution)/shard_map/ppermute | solution.py:17
  214.2 139.9 %reduce-scatter.5.cloned.1.call-start = ((), (), s32[]{:S(2)}) async-start(), calls=%async_computation.7 | async-start | bytes 3932160 | tf_op jit(solution)/shard_map/reduce_scatter | solution.py:33
  307.7 3.6 copy-start.6
  315.2 70.9 %all-gather.14.cloned.1.call-start = ((), (), s32[]{:S(2)}) async-start(), calls=%async_computation.8 | async-start | bytes 1966080 | tf_op jit(solution)/shard_map/all_gather | solution.py:69
  355.6 4.8 %collective-permute-start.1 = (bf16[256,30]{0,1:T(8,128)(2,1)S(1)}, bf16[256,30]{0,1:T(8,128)(2,1)S(1)}, u32[]{:S(2)}, u32[]{:S(2)}) collective-permute-start(bf16[256,30]{0,1:T(8,128)(2,1)S(1)} %slice.719), channel_id=1, source_target_pairs={{0,4},{4,8},{8,12},{12,16},{16,20},{20,24},{24,28},{1,5},{5,9},{9,... | collective-permute-start | bytes 46088 | tf_op jit(solution)/shard_map/ppermute | solution.py:17
Sparse Core Ops, SparseCore 0:
  9.4 77.3 all-gather.7
  88.8 72.8 all-gather.5
  167.2 35.8 reduce-scatter.2
  205.1 72.7 all-gather.11
  279.4 18.3 all-gather.9
  315.3 38.7 reduce-scatter.4
  365.3 20.6 all-gather.13
where the time goes:
time: 398 us
  waiting for transfers between devices  323 us (81%)
  matrix products  21.4 us (5%)
  other arithmetic  18.2 us (5%)
  blocking collectives  14.3 us (4%)
  between operations  13.7 us (3%)
  starting transfers between devices  7.01 us (2%)
    reduce_scatter x2, waiting for transfers between devices, gated_input(): lax.psum_scatter(jnp.stack([value_part, gate_part], axis=1).astype(jnp.bf...  74.1 us
    all_gather x1, waiting for transfers between devices, on_device(): lax.all_gather(value_proj, 'sp', axis=2, tiled=True)  71.4 us
    all_gather x1, waiting for transfers between devices, on_device(): lax.all_gather(gate_proj, 'sp', axis=2, tiled=True)  68.5 us
    all_gather x1, waiting for transfers between devices, on_device(): lax.all_gather(out_proj, 'sp', axis=1, tiled=True)  63.7 us
    all_gather x2, waiting for transfers between devices, project_out(): lax.all_gather(mixed, 'tp', axis=0, tiled=True)  40.6 us
    psum x2, blocking collectives, rms_normed(): squares = lax.psum(jnp.sum(wide_rows * wide_rows, axis=1), 'tp')  14.3 us
    dot_general x2, matrix products, project_out(): lax.dot_general(lax.all_gather(mixed, 'tp', axis=0, tiled=True), w_out, (...  9.1 us
  transfers between devices with their start and end apart: 9, of which 9 were waited for; matrix products, arithmetic and copies ran while one was open for 3% of the time, Pallas kernels for 0%

commit v1 on v0

--- a/solution.py
+++ b/solution.py
@@ -90,7 +90,7 @@
     group_size = C // GROUPS
     all_value, all_gate, all_out = (
         lax.all_gather(value_proj, "sp", axis=2, tiled=True),
-        lax.all_gather(gate_proj, "sp", axis=2, tiled=True),
+        jnp.concatenate(lax.all_gather(gate_proj, "sp"), axis=2),
         lax.all_gather(out_proj, "sp", axis=1, tiled=True),
     )
     residual_rows = hidden_in

time: 398 us -> 399 us (level)
  waiting for transfers between devices: 323 us -> 309 us
  local copies, waits for them, and re-layouts: 0.2 us -> 10.8 us
    slice x0 -> x3, local copies, waits for them, and re-layouts: none -> 10.6 us  [on_device(): w_value, w_gate, w_out = (all_value[level], all_gate[level], all_out[level])]
    all_gather x1, waiting for transfers between devices: 71.4 us -> 62.1 us  [on_device(): lax.all_gather(value_proj, 'sp', axis=2, tiled=True)]
  transfers between devices with their start and end apart: 9 -> 9, of which waited for: 9 -> 9; matrix products, arithmetic and copies ran while one was open for 3% -> 6% of each run, Pallas kernels for 0% -> 0%
where the time goes in v1:
time: 399 us; the launch traced here: 398 us
  waiting for transfers between devices  309 us (77%)
  matrix products  25 us (6%)
  other arithmetic  18.2 us (5%)
  blocking collectives  14.2 us (4%)
  between operations  13.8 us (3%)
  local copies, waits for them, and re-layouts  10.8 us (3%)
  starting transfers between devices  7.03 us (2%)
    reduce_scatter x2, waiting for transfers between devices, gated_input(): lax.psum_scatter(jnp.stack([value_part, gate_part], axis=1).astype(jnp.bf...  74.1 us
    all_gather x1, waiting for transfers between devices, on_device(): lax.all_gather(gate_proj, 'sp')  66.8 us
    all_gather x1, waiting for transfers between devices, on_device(): lax.all_gather(value_proj, 'sp', axis=2, tiled=True)  62.1 us
    all_gather x1, waiting for transfers between devices, on_device(): lax.all_gather(out_proj, 'sp', axis=1, tiled=True)  61 us
    all_gather x2, waiting for transfers between devices, project_out(): lax.all_gather(mixed, 'tp', axis=0, tiled=True)  40.6 us
    psum x2, blocking collectives, rms_normed(): squares = lax.psum(jnp.sum(wide_rows * wide_rows, axis=1), 'tp')  14.2 us
    slice x3, local copies, waits for them, and re-layouts, on_device(): w_value, w_gate, w_out = (all_value[level], all_gate[level], all_out[level])  10.6 us
    dot_general x2, matrix products, project_out(): lax.dot_general(lax.all_gather(mixed, 'tp', axis=0, tiled=True), w_out, (...  10.5 us
  transfers between devices with their start and end apart: 9, of which 9 were waited for; matrix products, arithmetic and copies ran while one was open for 6% of the time, Pallas kernels for 0%

profile of v1, /device:TPU:0, one launch (start us, length us, event | category | flops | bytes accessed | tf_op | source)
XLA Modules:
  0.0 398.4 jit_solution(14979419980086740624)
XLA Ops:
  6.5 0.7 all-gather.15.cloned.1.call-update
  8.1 1.8 fusion
  9.8 8.4 %psum.14 = f32[768]{0:T(1024)S(1)} all-reduce(f32[768]{0:T(1024)S(1)} %fusion), channel_id=1, replica_groups=mesh['sp'=8,'tp'=4] {'tp'}, use_global_device_ids=true, to_apply=%region_1.0 | all-reduce | flops 768 | bytes 6144 | tf_op jit(solution)/shard_map/psum | solution.py:22
  18.2 66.8 %all-gather.15.cloned.1.call-done = bf16[16,1024,128]{2,1,0:T(8,128)(2,1)} async-done(((bf16[2,1024,128]{2,1,0:T(8,128)(2,1)}), bf16[16,1024,128]{2,1,0:T(8,128)(2,1)}) %all-gather.15.cloned.1.call-update) | async-done | bytes 4194320 | tf_op jit(solution)/shard_map/all_gather | solution.py:93
  85.0 3.9 fusion.100
  89.0 3.9 copy.12
  92.9 5.2 %fusion.14 = bf16[1024,1,768]{0,2,1:T(8,128)(2,1)} fusion(bf16[1024,1024]{0,1:T(8,128)(2,1)} %bitcast.127, bf16[768,1024]{1,0:T(8,128)(2,1)} %param.9, f32[1024]{0:T(1024)S(1)} %bitcast.134, f32[768]{0:T(1024)S(1)} %add_rsqrt_fusion.3), kind=kOutput, calls=%fused_computation.28 | convolution fusion | flops 1614544896 | bytes 5250048 | tf_op jit(solution)/shard_map/dot_general | solution.py:32
  98.1 62.1 %all-gather.7.cloned.1.call-done = bf16[2,1024,1024]{2,1,0:T(8,128)(2,1)} async-done(((bf16[2,1024,128]{2,1,0:T(8,128)(2,1)}), bf16[2,1024,1024]{2,1,0:T(8,128)(2,1)}) %all-gather.7.cloned.1.call-update) | async-done | bytes 4194320 | tf_op jit(solution)/shard_map/all_gather | solution.py:92
  160.3 4.0 %fusion.17 = bf16[1024,1,768]{0,2,1:T(8,128)(2,1)S(1)} fusion(bf16[2,1024,1024]{2,1,0:T(8,128)(2,1)} %all-gather.7.cloned.1.call-done, bf16[768,1024]{1,0:T(8,128)(2,1)} %param.9, f32[1024]{0:T(1024)S(1)} %bitcast.135, f32[768]{0:T(1024)S(1)} %add_rsqrt_fusion.3), kind=kOutput, calls=%fused_computation.31 | convolution fusion | flops 1614544896 | bytes 5250048 | tf_op jit(solution)/shard_map/dot_general | solution.py:31
  164.3 2.0 pad_maximum_fusion
  167.2 35.2 %reduce-scatter.3.cloned.1.call-done = bf16[256,2,768]{0,2,1:T(8,128)(2,1)} async-done(((bf16[1024,2,768]{0,2,1:T(8,128)(2,1)}), bf16[256,2,768]{0,2,1:T(8,128)(2,1)}) %reduce-scatter.3.cloned.1.call-update) | async-done | bytes 786448 | tf_op jit(solution)/shard_map/reduce_scatter | solution.py:33
  202.4 1.2 convert_element_type.123
  203.9 3.4 collective-permute-start
  207.3 1.4 collective-permute-done
  208.8 3.3 fusion.98
  212.4 1.1 multiply_convert_fusion.1
  213.5 2.7 copy.13
  216.3 61.0 %all-gather.11.cloned.1.call-done = bf16[2,1024,1024]{2,1,0:T(8,128)(2,1)} async-done(((bf16[2,128,1024]{2,1,0:T(8,128)(2,1)}), bf16[2,1024,1024]{2,1,0:T(8,128)(2,1)}) %all-gather.11.cloned.1.call-update) | async-done | bytes 4194320 | tf_op jit(solution)/shard_map/all_gather | solution.py:94
  277.2 19.8 %all-gather.9.cloned.1.call-done = bf16[1024,768]{0,1:T(8,128)(2,1)} async-done(((bf16[256,768]{0,1:T(8,128)(2,1)}), bf16[1024,768]{0,1:T(8,128)(2,1)}) %all-gather.9.cloned.1.call-update) | async-done | bytes 1572880 | tf_op jit(solution)/shard_map/all_gather | solution.py:69
  297.0 5.5 %fusion.4 = (f32[768]{0:T(1024)S(1)}, bf16[768,1024]{1,0:T(8,128)(2,1)}) fusion(bf16[1024,768]{0,1:T(8,128)(2,1)} %all-gather.9.cloned.1.call-done, bf16[2,1024,1024]{2,1,0:T(8,128)(2,1)} %all-gather.11.cloned.1.call-done, bf16[768,1024]{1,0:T(8,128)(2,1)} %param.9), kind=kOutput, calls=%fused_computation.10 | convolution fusion | flops 1615330560 | bytes 6818816 | tf_op jit(solution)/shard_map/dot_general | solution.py:68
  302.5 5.9 %psum.15 = f32[768]{0:T(1024)S(1)} all-reduce(f32[768]{0:T(1024)S(1)} %get-tuple-element.83), channel_id=1, replica_groups=mesh['sp'=8,'tp'=4] {'tp'}, use_global_device_ids=true, to_apply=%region_6.7 | all-reduce | flops 768 | bytes 6144 | tf_op jit(solution)/shard_map/psum | solution.py:22
  308.4 3.4 fusion.15
  311.9 1.8 fusion.16
  313.7 1.9 pad_maximum_fusion.1
  315.7 38.9 %reduce-scatter.5.cloned.1.call-done = bf16[256,2,768]{0,2,1:T(8,128)(2,1)} async-done(((bf16[1024,2,768]{0,2,1:T(8,128)(2,1)}), bf16[256,2,768]{0,2,1:T(8,128)(2,1)}) %reduce-scatter.5.cloned.1.call-update) | async-done | bytes 786448 | tf_op jit(solution)/shard_map/reduce_scatter | solution.py:33
  354.6 1.2 convert_element_type.137
  356.1 3.4 collective-permute-start.1
  359.5 1.4 collective-permute-done.1
  361.0 3.3 fusion.96
  364.6 1.1 multiply_convert_fusion
  365.7 20.8 %all-gather.13.cloned.1.call-done = bf16[1024,768]{0,1:T(8,128)(2,1)} async-done(((bf16[256,768]{0,1:T(8,128)(2,1)}), bf16[1024,768]{0,1:T(8,128)(2,1)}) %all-gather.13.cloned.1.call-update) | async-done | bytes 1572880 | tf_op jit(solution)/shard_map/all_gather | solution.py:69
  386.5 5.0 %fusion.7 = bf16[768,1024]{1,0:T(8,128)(2,1)} fusion(bf16[768,1024]{1,0:T(8,128)(2,1)S(1)} %copy-done.9, bf16[1024,768]{0,1:T(8,128)(2,1)} %all-gather.13.cloned.1.call-done, bf16[2,1024,1024]{2,1,0:T(8,128)(2,1)} %all-gather.11.cloned.1.call-done), kind=kOutput, calls=%fused_computation.13 | convolution fusion | flops 1612972032 | bytes 6815744 | tf_op jit(solution)/shard_map/dot_general | solution.py:68
  (56 shorter events, 3.0 us)
Async XLA Ops:
  6.5 11.7 %copy-start.3 = (bf16[2,1024]{1,0:T(2,128)(2,1)S(1)}, bf16[2,1024]{1,0:T(2,128)(2,1)}, u32[]{:S(2)}) copy-start(bf16[2,1024]{1,0:T(2,128)(2,1)} %param.10) | copy-start | bytes 12292
  6.5 78.5 %all-gather.15.cloned.1.call-start = ((), (), s32[]{:S(2)}) async-start(), calls=%async_computation.8 | async-start | bytes 4718592 | tf_op jit(solution)/shard_map/all_gather | solution.py:93
  7.3 153.0 %all-gather.7.cloned.1.call-start = ((), (), s32[]{:S(2)}) async-start(), calls=%async_computation.2 | async-start | bytes 4718592 | tf_op jit(solution)/shard_map/all_gather | solution.py:92
  8.0 194.4 %reduce-scatter.3.cloned.1.call-start = ((), (), s32[]{:S(2)}) async-start(), calls=%async_computation.3 | async-start | bytes 3932160 | tf_op jit(solution)/shard_map/reduce_scatter | solution.py:33
  160.3 4.0 %copy-start.1 = (bf16[1024,1,768]{0,2,1:T(8,128)(2,1)S(1)}, bf16[1024,1,768]{0,2,1:T(8,128)(2,1)}, u32[]{:S(2)}) copy-start(bf16[1024,1,768]{0,2,1:T(8,128)(2,1)} %fusion.14) | copy-start | bytes 4718596
  166.3 0.7 copy-start.4
  166.3 0.7 copy-start.5
  166.3 0.8 copy-start.2
  166.3 110.9 %all-gather.11.cloned.1.call-start = ((), (), s32[]{:S(2)}) async-start(), calls=%async_computation.5 | async-start | bytes 4718592 | tf_op jit(solution)/shard_map/all_gather | solution.py:94
  166.9 130.1 %all-gather.9.cloned.1.call-start = ((), (), s32[]{:S(2)}) async-start(), calls=%async_computation.4 | async-start | bytes 1966080 | tf_op jit(solution)/shard_map/all_gather | solution.py:69
  167.2 40.1 %copy-start.6 = (bf16[2,256]{1,0:T(2,128)(2,1)S(1)}, bf16[2,256]{1,0:T(2,128)(2,1)}, u32[]{:S(2)}) copy-start(bf16[2,256]{1,0:T(2,128)(2,1)} %param.16) | copy-start | bytes 3076
  203.9 4.8 %collective-permute-start = (bf16[256,30]{0,1:T(8,128)(2,1)S(1)}, bf16[256,30]{0,1:T(8,128)(2,1)S(1)}, u32[]{:S(2)}, u32[]{:S(2)}) collective-permute-start(bf16[256,30]{0,1:T(8,128)(2,1)S(1)} %slice.653), channel_id=1, source_target_pairs={{0,4},{4,8},{8,12},{12,16},{16,20},{20,24},{24,28},{1,5},{5,9},{9,... | collective-permute-start | bytes 46088 | tf_op jit(solution)/shard_map/ppermute | solution.py:17
  213.5 141.1 %reduce-scatter.5.cloned.1.call-start = ((), (), s32[]{:S(2)}) async-start(), calls=%async_computation.6 | async-start | bytes 3932160 | tf_op jit(solution)/shard_map/reduce_scatter | solution.py:33
  216.3 92.2 %copy-start = (bf16[1,1024,8,128]{1,3,2,0:T(8,128)(2,1)S(1)}, bf16[1,1024,8,128]{1,3,2,0:T(8,128)(2,1)}, u32[]{:S(2)}) copy-start(bf16[1,1024,8,128]{1,3,2,0:T(8,128)(2,1)} %copy.13) | copy-start | bytes 6291460
  308.4 3.4 copy-start.7
  308.4 3.4 copy-start.8
  315.7 70.9 %all-gather.13.cloned.1.call-start = ((), (), s32[]{:S(2)}) async-start(), calls=%async_computation.7 | async-start | bytes 1966080 | tf_op jit(solution)/shard_map/all_gather | solution.py:69
  356.1 4.8 %collective-permute-start.1 = (bf16[256,30]{0,1:T(8,128)(2,1)S(1)}, bf16[256,30]{0,1:T(8,128)(2,1)S(1)}, u32[]{:S(2)}, u32[]{:S(2)}) collective-permute-start(bf16[256,30]{0,1:T(8,128)(2,1)S(1)} %slice.721), channel_id=1, source_target_pairs={{0,4},{4,8},{8,12},{12,16},{16,20},{20,24},{24,28},{1,5},{5,9},{9,... | collective-permute-start | bytes 46088 | tf_op jit(solution)/shard_map/ppermute | solution.py:17
  364.3 22.2 %copy-start.9 = (bf16[768,1024]{1,0:T(8,128)(2,1)S(1)}, bf16[768,1024]{1,0:T(8,128)(2,1)}, u32[]{:S(2)}) copy-start(bf16[768,1024]{1,0:T(8,128)(2,1)} %get-tuple-element.84) | copy-start | bytes 4718596
Sparse Core Ops, SparseCore 0:
  9.5 75.5 all-gather.14
  87.0 73.1 all-gather.6
  166.4 35.8 reduce-scatter.2
  204.4 72.7 all-gather.10
  278.6 18.3 all-gather.8
  315.8 38.7 reduce-scatter.4
  365.9 20.6 all-gather.12
